TPU v7x, 32 devices: a whole 2x2x4 slice. The times are simulated.
32 devices in a mesh: ep: 16 (over z, y, x), tp: 2 (over core).
Axes of the slice: x: 2, y: 2, z: 4, core: 2. Of those that a mesh axis runs over, the one named last changes fastest.
Arguments:
- tokens: bfloat16 [512, 2048], P('ep'), may hold values from -6 to 6
- mix_gain: float32 [2048], replicated, may hold values from 0.1 to 1.9
- w_query: bfloat16 [2048, 512], P('ep', 'tp'), may hold values from -0.125 to 0.125
- w_key: bfloat16 [2048, 512], P('ep', 'tp'), may hold values from -0.125 to 0.125
- w_value: bfloat16 [2048, 512], P('ep', 'tp'), may hold values from -0.125 to 0.125
- w_outgate: bfloat16 [2048, 512], P('ep', 'tp'), may hold values from -0.125 to 0.125
- w_igate: bfloat16 [2048, 8], P('ep', 'tp'), may hold values from -0.125 to 0.125
- w_fgate: bfloat16 [2048, 8], P('ep', 'tp'), may hold values from -0.125 to 0.125
- igate_bias: float32 [8], P('tp'), may hold values from -2 to 1
- fgate_bias: float32 [8], P('tp'), may hold values from 0 to 4
- head_gain: float32 [512], P('tp'), may hold values from 0.1 to 1.9
- w_out: bfloat16 [512, 2048], P('tp', 'ep'), may hold values from -0.25 to 0.25
- state_matrix: float32 [512, 8, 64, 64], P('ep', 'tp'), may hold values from -2.4 to 2.4
- state_norm: float32 [512, 8, 64], P('ep', 'tp'), may hold values from -2.4 to 2.4
- state_max: float32 [512, 8], P('ep', 'tp'), may hold values from -4 to 4
- ffn_gain: float32 [2048], replicated, may hold values from 0.1 to 1.9
- w_expert_gate: bfloat16 [16, 2048, 1408], P('ep', None, 'tp'), may hold values from -0.125 to 0.125
- w_expert_up: bfloat16 [16, 2048, 1408], P('ep', None, 'tp'), may hold values from -0.125 to 0.125
- w_expert_down: bfloat16 [16, 1408, 2048], P('ep', 'tp'), may hold values from -0.15625 to 0.15625
- routes: int32 [512, 3], P('ep'), may hold values from 0 to 15, all different within a row; in each aligned block of 32 rows (0 to 31, 32 to 63, ...) at most 12 rows name the same one
- route_weights: float32 [512, 3], P('ep'), may hold values from 0.2 to 1
Outputs:
- mixed: bfloat16 [512, 2048], P('ep')
- new_matrix: float32 [512, 8, 64, 64], P('ep', 'tp')
- new_norm: float32 [512, 8, 64], P('ep', 'tp')
- new_max: float32 [512, 8], P('ep', 'tp')
Inputs may be any that keep to these rules, and one draw needn't show every extreme that they name: `routes`: each row names 3 different experts. Among the rows of one device, no expert is named by more than 12 rows, a bound that some block reaches.
All inputs are finite; a program needn't handle non-finite values.
Results may differ from a plain program's by a relative error of at most 0.017.
Values may be sent and summed in bfloat16 or wider, within the bound.
No kernel may reach another device: no remote copies, remote signals or barrier semaphores. Data moves between devices by JAX's collectives and lax.ppermute only.
A program may use at most 128 MiB of HBM per device.

v0:
```python
import jax
import jax.numpy as jnp
from jax import lax
from jax.sharding import PartitionSpec as P


def rms_scale(values_in, gain_vec):
    widened = values_in.astype(jnp.float32)
    return (
        widened * lax.rsqrt(jnp.mean(widened * widened, axis=-1, keepdims=True) + 1e-06) * gain_vec
    )


def memory_cell(
    query,
    key_row,
    value_row,
    outgate,
    input_pre,
    forget_pre,
    head_gain,
    state_matrix,
    state_norm,
    state_max,
):
    seq_rows, head_count = input_pre.shape
    head_size = query.shape[1] // head_count
    query_heads = query.astype(jnp.float32).reshape(seq_rows, head_count, head_size)
    key_heads = key_row.astype(jnp.float32).reshape(
        seq_rows, head_count, head_size
    ) * head_size ** (-0.5)
    value_heads = value_row.astype(jnp.float32).reshape(seq_rows, head_count, head_size)
    log_forget = jax.nn.log_sigmoid(forget_pre)
    new_max = jnp.maximum(log_forget + state_max, input_pre)
    keep_old = jnp.exp(log_forget + state_max - new_max)
    keep_new = jnp.exp(input_pre - new_max)
    new_matrix = (
        keep_old[:, :, None, None] * state_matrix
        + keep_new[:, :, None, None] * value_heads[:, :, :, None] * key_heads[:, :, None, :]
    )
    new_norm = keep_old[:, :, None] * state_norm + keep_new[:, :, None] * key_heads
    numerator = jnp.einsum(
        "bhvd,bhd->bhv", new_matrix, query_heads, precision=lax.Precision.HIGHEST
    )
    denominator = jnp.sum(new_norm * query_heads, axis=-1)
    cell_read = numerator / jnp.maximum(jnp.abs(denominator), jnp.exp(-new_max))[:, :, None]
    centered = cell_read - jnp.mean(cell_read, axis=-1, keepdims=True)
    variance = jnp.mean(centered * centered, axis=-1, keepdims=True)
    scaled_cell = (centered * lax.rsqrt(variance + 1e-06)).reshape(seq_rows, head_count * head_size)
    cell_out = (scaled_cell * head_gain * jax.nn.sigmoid(outgate.astype(jnp.float32))).astype(
        jnp.bfloat16
    )
    return (cell_out, new_matrix, new_norm, new_max)


def body(
    tokens,
    mix_gain,
    w_query,
    w_key,
    w_value,
    w_outgate,
    w_igate,
    w_fgate,
    igate_bias,
    fgate_bias,
    head_gain,
    w_out,
    state_matrix,
    state_norm,
    state_max,
    ffn_gain,
    w_expert_gate,
    w_expert_up,
    w_expert_down,
    routes,
    route_weights,
):
    seq_rows, width = tokens.shape
    normed = rms_scale(tokens, mix_gain).astype(jnp.bfloat16)
    weight_list = (w_query, w_key, w_value, w_outgate, w_igate, w_fgate)
    spread = lax.all_to_all(normed, "ep", split_axis=1, concat_axis=0, tiled=True)
    joined = jnp.concatenate(weight_list, axis=1)
    summed = lax.psum_scatter(
        jnp.dot(spread, joined, preferred_element_type=jnp.float32),
        "ep",
        scatter_dimension=0,
        tiled=True,
    )
    bounds = [0]
    for weight in weight_list:
        bounds.append(bounds[-1] + weight.shape[1])
    projected = tuple(
        (summed[:, bounds[index] : bounds[index + 1]] for index in range(len(weight_list)))
    )
    query = projected[0].astype(jnp.bfloat16)
    key_row = projected[1].astype(jnp.bfloat16)
    value_row = projected[2].astype(jnp.bfloat16)
    outgate = projected[3].astype(jnp.bfloat16)
    input_pre = projected[4] + igate_bias
    forget_pre = projected[5] + fgate_bias
    cell_out, new_matrix, new_norm, new_max = memory_cell(
        query,
        key_row,
        value_row,
        outgate,
        input_pre,
        forget_pre,
        head_gain,
        state_matrix,
        state_norm,
        state_max,
    )
    partial_out = jnp.dot(
        cell_out,
        lax.all_gather(w_out, "ep", axis=1, tiled=True),
        preferred_element_type=jnp.float32,
    )
    attended = lax.psum(partial_out.astype(jnp.bfloat16), "tp").astype(jnp.float32)
    resid = (tokens.astype(jnp.float32) + attended).astype(jnp.bfloat16)
    normed_two = rms_scale(resid, ffn_gain).astype(jnp.bfloat16)
    ep_count = lax.axis_size("ep")
    local_experts = w_expert_gate.shape[0]
    expert_total = local_experts * ep_count
    top_count = routes.shape[1]
    capacity = max(2, 2 * seq_rows * top_count // expert_total)
    flat_routes = routes.reshape(-1)
    onehot = (flat_routes[:, None] == jnp.arange(expert_total, dtype=jnp.int32)[None, :]).astype(
        jnp.int32
    )
    earlier = jnp.cumsum(onehot, axis=0, dtype=jnp.int32) - onehot
    slots = jnp.sum(onehot * earlier, axis=1, dtype=jnp.int32)
    targets = flat_routes * capacity + slots
    dispatch = (
        targets[:, None] == jnp.arange(expert_total * capacity, dtype=jnp.int32)[None, :]
    ).astype(jnp.bfloat16)
    route_rows = jnp.repeat(normed_two, top_count, axis=0)
    outgoing = jnp.einsum(
        "rs,rd->sd", dispatch, route_rows, preferred_element_type=jnp.float32
    ).astype(jnp.bfloat16)
    outgoing = outgoing.reshape(expert_total, capacity, width)
    received = lax.all_to_all(outgoing, "ep", split_axis=0, concat_axis=0, tiled=True)
    slot_count = received.shape[1]
    regrouped = received.reshape(ep_count, local_experts, slot_count, width)
    gate_pre = jnp.einsum(
        "nxcd,xdf->nxcf", regrouped, w_expert_gate, preferred_element_type=jnp.float32
    )
    up_pre = jnp.einsum(
        "nxcd,xdf->nxcf", regrouped, w_expert_up, preferred_element_type=jnp.float32
    )
    hidden = (jax.nn.silu(gate_pre) * up_pre).astype(jnp.bfloat16)
    partial_down = jnp.einsum(
        "nxcf,xfd->nxcd", hidden, w_expert_down, preferred_element_type=jnp.float32
    )
    expert_sum = lax.psum(partial_down.astype(jnp.bfloat16), "tp")
    finished = expert_sum.reshape(ep_count * local_experts, slot_count, width)
    returned = lax.all_to_all(finished, "ep", split_axis=0, concat_axis=0, tiled=True)
    picked = jnp.dot(
        dispatch,
        returned.reshape(expert_total * capacity, width),
        preferred_element_type=jnp.float32,
    )
    weighted = jnp.sum(
        picked.reshape(seq_rows, top_count, width) * route_weights[:, :, None], axis=1
    )
    mixed = (resid.astype(jnp.float32) + weighted).astype(jnp.bfloat16)
    return (mixed, new_matrix, new_norm, new_max)


def solution(mesh):
    placed = (
        P("ep", None),
        P(),
        P("ep", "tp"),
        P("ep", "tp"),
        P("ep", "tp"),
        P("ep", "tp"),
        P("ep", "tp"),
        P("ep", "tp"),
        P("tp"),
        P("tp"),
        P("tp"),
        P("tp", "ep"),
        P("ep", "tp", None, None),
        P("ep", "tp", None),
        P("ep", "tp"),
        P(),
        P("ep", None, "tp"),
        P("ep", None, "tp"),
        P("ep", "tp", None),
        P("ep", None),
        P("ep", None),
    )
    return jax.shard_map(
        body,
        mesh=mesh,
        in_specs=placed,
        out_specs=(P("ep", None), P("ep", "tp", None, None), P("ep", "tp", None), P("ep", "tp")),
        check_vma=False,
    )
```

profile of v0, /device:TPU:8, one launch (start us, length us, event | category | flops | bytes accessed | tf_op | source)
XLA Modules:
  0.0 342.0 jit_solution(8380659892496630698)
XLA Ops:
  7.2 0.0 copy-start
  7.2 1.2 fusion.36
  8.4 1.7 copy_bitcast_fusion
  10.1 7.2 %all-to-all-start = ((bf16[32,16,128]{2,0,1:T(8,128)(2,1)}), bf16[32,16,128]{2,0,1:T(8,128)(2,1)S(1)}, u32[]{:S(2)}, u32[]{:S(2)}) async-start(bf16[32,16,128]{2,0,1:T(8,128)(2,1)} %copy_bitcast_fusion), calls=%async_computation | async-start | bytes 262144 | tf_op jit(solution)/shard_map/all_to_all | solution.py:82
  17.3 0.0 reduce-scatter.2.cloned.1.call-start
  17.3 0.8 copy.58
  18.1 0.8 copy.59
  19.0 1.1 concatenate.3
  20.0 3.9 %all-to-all-done = bf16[32,16,128]{2,0,1:T(8,128)(2,1)S(1)} async-done(((bf16[32,16,128]{2,0,1:T(8,128)(2,1)}), bf16[32,16,128]{2,0,1:T(8,128)(2,1)S(1)}, u32[]{:S(2)}, u32[]{:S(2)}) %all-to-all-start) | async-done | bytes 131104 | tf_op jit(solution)/shard_map/all_to_all | solution.py:82
  23.9 1.9 fusion.62
  25.8 0.0 reduce-scatter.2.cloned.1.call-update
  25.8 0.0 all-gather.2.cloned.1.call-start
  25.8 0.7 all-gather.2.cloned.1.call-update
  26.5 0.0 all-reduce.3.cloned.1.call-start
  26.6 0.1 copy.60
  26.7 0.1 copy.61
  26.8 0.1 eq.50
  26.9 0.1 fusion.49
  27.0 0.1 reduce_window_sum.11
  27.1 0.2 select_reduce_fusion
  27.3 125.7 %reduce-scatter.2.cloned.1.call-done = f32[32,1032]{1,0:T(8,128)} async-done(((f32[512,1032]{1,0:T(8,128)}), f32[32,1032]{1,0:T(8,128)}) %reduce-scatter.2.cloned.1.call-update) | async-done | bytes 132112 | tf_op jit(solution)/shard_map/reduce_scatter | solution.py:84
  153.0 0.9 convert.9
  154.0 0.1 reshape.150
  154.1 0.1 reshape.171
  154.1 0.1 reshape.163
  154.2 0.1 reshape.161
  154.4 0.9 broadcast_multiply_fusion.3
  155.3 0.8 subtract_exponential_fusion.1
  156.1 0.8 multiply_reduce_fusion.1
  156.9 3.8 %multiply_add_fusion = f32[32,4,64,64]{3,2,1,0:T(8,128)S(1)} fusion(f32[32,4,64,64]{3,2,1,0:T(8,128)} %param.33, f32[32,4,64]{2,1,0:T(4,128)S(1)} %get-tuple-element.30, f32[32,4,64]{2,1,0:T(4,128)S(1)} %get-tuple-element.31, f32[32,4]{1,0:T(8,128)S(1)} %subtract_exponential_fusion.1), kind=kLoop, calls=%fused_computation | loop fusion | flops 1572864 | bytes 4260352 | tf_op jit(solution)/shard_map/add | solution.py:38
  160.7 0.0 copy-start.1
  160.7 2.0 copy-done.1
  162.7 3.4 fusion.63
  166.1 0.2 fusion.59
  166.3 0.2 multiply_reduce_fusion
  166.5 0.1 subtract_multiply_fusion
  166.6 0.1 reshape.152
  166.7 39.0 %all-gather.2.cloned.1.call-done = bf16[256,2048]{1,0:T(8,128)(2,1)} async-done(((bf16[256,128]{1,0:T(8,128)(2,1)}), bf16[256,2048]{1,0:T(8,128)(2,1)}) %all-gather.2.cloned.1.call-update) | async-done | bytes 1048592 | tf_op jit(solution)/shard_map/all_gather | solution.py:116
  205.7 2.2 convolution_convert_fusion.1
  207.8 0.0 all-reduce.3.cloned.1.call-update
  207.9 0.0 all-reduce.5.cloned.1.call-start
  207.9 0.5 multiply_add_fusion.3
  208.4 18.1 %all-reduce.3.cloned.1.call-done = bf16[32,2048]{1,0:T(8,128)(2,1)} async-done(((bf16[32,2048]{1,0:T(8,128)(2,1)}), bf16[32,2048]{1,0:T(8,128)(2,1)}) %all-reduce.3.cloned.1.call-update) | async-done | bytes 131088 | tf_op jit(solution)/shard_map/psum | solution.py:119
  226.5 1.1 fusion.40
  227.6 1.0 fusion.42
  228.6 0.2 broadcast_in_dim.2
  228.8 1.1 reshape.153
  229.9 2.4 convolution_convert_fusion
  232.3 2.1 reshape.154
  234.4 33.1 %all_to_all.29 = bf16[16,12,2048]{2,1,0:T(8,128)(2,1)S(1)} all-to-all(bf16[16,12,2048]{2,1,0:T(8,128)(2,1)} %reshape.154), channel_id=1, replica_groups=mesh['ep'=16,'tp'=2] {'ep'}, dimensions={0} | all-to-all | bytes 1572864 | tf_op jit(solution)/shard_map/all_to_all | solution.py:142
  267.5 1.0 copy-done.4
  268.5 3.8 %fusion.9 = f32[16,1,12,704]{3,0,2,1:T(8,128)} fusion(bf16[1,2048,704]{1,2,0:T(8,128)(2,1)} %param.37, bf16[16,12,2048]{2,1,0:T(8,128)(2,1)S(1)} %all_to_all.29), kind=kOutput, calls=%fused_computation.11 | convolution fusion | flops 553648128 | bytes 4210688 | tf_op jit(solution)/shard_map/nxcd,xdf->nxcf/dot_general | solution.py:145
  272.3 5.2 %fusion.6 = bf16[16,12,2048]{2,0,1:T(8,128)(2,1)} fusion(bf16[1,704,2048]{2,1,0:T(8,128)(2,1)S(1)} %copy-done, bf16[1,2048,704]{1,2,0:T(8,128)(2,1)} %param.38, f32[16,1,12,704]{3,0,2,1:T(8,128)} %fusion.9, bf16[16,12,2048]{2,1,0:T(8,128)(2,1)} %copy-done.4), kind=kOutput, calls=%fused_computation.7 | convolution fusion | flops 1108500480 | bytes 7880704 | tf_op jit(solution)/shard_map/nxcf,xfd->nxcd/dot_general | solution.py:152
  277.5 0.0 all-reduce.5.cloned.1.call-update
  277.6 17.9 %all-reduce.5.cloned.1.call-done = bf16[16,12,2048]{2,0,1:T(8,128)(2,1)} async-done(((bf16[16,12,2048]{2,0,1:T(8,128)(2,1)}), bf16[16,12,2048]{2,0,1:T(8,128)(2,1)}) %all-reduce.5.cloned.1.call-update) | async-done | bytes 786448 | tf_op jit(solution)/shard_map/psum | solution.py:155
  295.5 2.6 copy.65
  298.1 7.1 %all-to-all-start.2 = ((bf16[16,12,2048]{2,1,0:T(8,128)(2,1)}), bf16[16,12,2048]{2,1,0:T(8,128)(2,1)}, u32[]{:S(2)}, u32[]{:S(2)}) async-start(bf16[16,12,2048]{2,1,0:T(8,128)(2,1)} %copy.65), calls=%async_computation.3 | async-start | bytes 2097152 | tf_op jit(solution)/shard_map/all_to_all | solution.py:157
  305.2 0.1 reduce_sum.70
  305.3 0.1 copy.62
  305.4 0.7 copy.66
  306.0 25.1 %all-to-all-done.2 = bf16[16,12,2048]{2,1,0:T(8,128)(2,1)} async-done(((bf16[16,12,2048]{2,1,0:T(8,128)(2,1)}), bf16[16,12,2048]{2,1,0:T(8,128)(2,1)}, u32[]{:S(2)}, u32[]{:S(2)}) %all-to-all-start.2) | async-done | bytes 786464 | tf_op jit(solution)/shard_map/all_to_all | solution.py:157
  331.1 2.1 reshape.169
  333.2 1.5 fusion.18
  334.7 0.7 fusion.43
  (35 shorter events, 0.1 us)
Async XLA Ops:
  7.2 265.2 %copy-start = (bf16[1,704,2048]{2,1,0:T(8,128)(2,1)S(1)}, bf16[1,704,2048]{2,1,0:T(8,128)(2,1)}, u32[]{:S(2)}) copy-start(bf16[1,704,2048]{2,1,0:T(8,128)(2,1)} %param.39) | copy-start | bytes 8650756
  10.1 13.8 %all-to-all-start = ((bf16[32,16,128]{2,0,1:T(8,128)(2,1)}), bf16[32,16,128]{2,0,1:T(8,128)(2,1)S(1)}, u32[]{:S(2)}, u32[]{:S(2)}) async-start(bf16[32,16,128]{2,0,1:T(8,128)(2,1)} %copy_bitcast_fusion), calls=%async_computation | async-start | bytes 262144 | tf_op jit(solution)/shard_map/all_to_all | solution.py:82
  17.3 135.7 %reduce-scatter.2.cloned.1.call-start = ((), (), s32[]{:S(2)}) async-start(), calls=%async_computation.4 | async-start | bytes 2506752 | tf_op jit(solution)/shard_map/reduce_scatter | solution.py:84
  18.9 7.6 %copy-start.13 = (f32[32,4]{0,1:T(4,128)S(1)}, f32[32,4]{0,1:T(4,128)}, u32[]{:S(2)}) copy-start(f32[32,4]{0,1:T(4,128)} %param.35) | copy-start | bytes 1540
  18.9 7.7 %copy-start.7 = (s32[32,3]{0,1:T(4,128)S(1)}, s32[32,3]{0,1:T(4,128)}, u32[]{:S(2)}) copy-start(s32[32,3]{0,1:T(4,128)} %param.40) | copy-start | bytes 1156
  23.9 130.5 %copy-start.10 = (f32[4]{0:T(128)S(1)}, f32[4]{0:T(128)}, u32[]{:S(2)}) copy-start(f32[4]{0:T(128)} %param.30) | copy-start | bytes 52
  23.9 130.5 %copy-start.15 = (f32[4]{0:T(128)S(1)}, f32[4]{0:T(128)}, u32[]{:S(2)}) copy-start(f32[4]{0:T(128)} %param.29) | copy-start | bytes 52
  23.9 132.2 %copy-start.5 = (f32[32,4,64]{2,1,0:T(4,128)S(1)}, f32[32,4,64]{2,1,0:T(4,128)}, u32[]{:S(2)}) copy-start(f32[32,4,64]{2,1,0:T(4,128)} %param.34) | copy-start | bytes 98308
  25.8 179.9 %all-gather.2.cloned.1.call-start = ((), (), s32[]{:S(2)}) async-start(), calls=%async_computation.5 | async-start | bytes 1114112 | tf_op jit(solution)/shard_map/all_gather | solution.py:116
  26.5 200.0 %all-reduce.3.cloned.1.call-start = ((), (), s32[]{:S(2)}) async-start(), calls=%async_computation.6 | async-start | bytes 262144 | tf_op jit(solution)/shard_map/psum | solution.py:119
  27.3 180.6 %copy-start.11 = (s32[96]{0:T(128)}, s32[96]{0:T(128)S(1)}, u32[]{:S(2)}) copy-start(s32[96]{0:T(128)S(1)} %select_reduce_fusion) | copy-start | bytes 1156
  160.7 2.0 copy-start.1
  162.7 43.0 %copy-start.14 = (f32[256]{0:T(256)S(1)}, f32[256]{0:T(256)}, u32[]{:S(2)}) copy-start(f32[256]{0:T(256)} %param.31) | copy-start | bytes 3076
  162.7 63.8 %copy-start.2 = (bf16[32,2048]{1,0:T(8,128)(2,1)S(1)}, bf16[32,2048]{1,0:T(8,128)(2,1)}, u32[]{:S(2)}) copy-start(bf16[32,2048]{1,0:T(8,128)(2,1)} %param.21) | copy-start | bytes 393220
  162.7 64.9 %copy-start.6 = (f32[2048]{0:T(1024)S(1)}, f32[2048]{0:T(1024)}, u32[]{:S(2)}) copy-start(f32[2048]{0:T(1024)} %param.36) | copy-start | bytes 24580
  207.9 87.6 %all-reduce.5.cloned.1.call-start = ((), (), s32[]{:S(2)}) async-start(), calls=%async_computation.7 | async-start | bytes 1572864 | tf_op jit(solution)/shard_map/psum | solution.py:155
  267.5 1.0 copy-start.4
  277.5 27.7 %copy-start.12 = (s32[96]{0:T(128)S(1)}, s32[96]{0:T(128)}, u32[]{:S(2)}) copy-start(s32[96]{0:T(128)} %copy-done.11) | copy-start | bytes 1156
  277.5 27.8 %copy-start.8 = (s32[32,3]{0,1:T(4,128)S(1)}, s32[32,3]{0,1:T(4,128)}, u32[]{:S(2)}) copy-start(s32[32,3]{0,1:T(4,128)} %param.40) | copy-start | bytes 1156
  277.6 55.7 %copy-start.9 = (f32[32,3]{0,1:T(4,128)S(1)}, f32[32,3]{0,1:T(4,128)}, u32[]{:S(2)}) copy-start(f32[32,3]{0,1:T(4,128)} %param.41) | copy-start | bytes 1156
  298.1 36.6 %copy-start.3 = (bf16[32,2048]{1,0:T(8,128)(2,1)S(1)}, bf16[32,2048]{1,0:T(8,128)(2,1)}, u32[]{:S(2)}) copy-start(bf16[32,2048]{1,0:T(8,128)(2,1)} %all-reduce.3.cloned.1.call-done) | copy-start | bytes 393220
  298.1 33.0 %all-to-all-start.2 = ((bf16[16,12,2048]{2,1,0:T(8,128)(2,1)}), bf16[16,12,2048]{2,1,0:T(8,128)(2,1)}, u32[]{:S(2)}, u32[]{:S(2)}) async-start(bf16[16,12,2048]{2,1,0:T(8,128)(2,1)} %copy.65), calls=%async_computation.3 | async-start | bytes 2097152 | tf_op jit(solution)/shard_map/all_to_all | solution.py:157
Sparse Core Ops, SparseCore 0:
  25.9 127.0 reduce-scatter.1
  155.7 49.9 all-gather.1
  208.6 17.9 all-reduce.2
  277.7 17.7 all-reduce.4
where the time goes:
time: 343 us; the launch traced here: 342 us
  waiting for transfers between devices  230 us (67%)
  blocking collectives  33.1 us (10%)
  matrix products  20.2 us (6%)
  local copies, waits for them, and re-layouts  15.4 us (4%)
  starting transfers between devices  14.5 us (4%)
  other arithmetic  14.3 us (4%)
  between operations  14 us (4%)
    reduce_scatter x1, waiting for transfers between devices, body(): lax.psum_scatter(jnp.dot(spread, joined, preferred_element_type=jnp.float...  126 us
    all_gather x1, waiting for transfers between devices, body(): lax.all_gather(w_out, 'ep', axis=1, tiled=True)  39 us
    all_to_all x1, blocking collectives, body(): lax.all_to_all(outgoing, 'ep', split_axis=0, concat_axis=0, tiled=True)  33.1 us
    all_to_all x1, waiting for transfers between devices, body(): lax.all_to_all(finished, 'ep', split_axis=0, concat_axis=0, tiled=True)  25.1 us
    psum x1, waiting for transfers between devices, body(): lax.psum(partial_out.astype(jnp.bfloat16), 'tp').astype(jnp.float32)  18.1 us
    psum x1, waiting for transfers between devices, body(): expert_sum = lax.psum(partial_down.astype(jnp.bfloat16), 'tp')  17.9 us
    all_to_all x1, starting transfers between devices, body(): lax.all_to_all(normed, 'ep', split_axis=1, concat_axis=0, tiled=True)  7.22 us
    all_to_all x1, starting transfers between devices, body(): lax.all_to_all(finished, 'ep', split_axis=0, concat_axis=0, tiled=True)  7.11 us
  transfers between devices with their start and end apart: 6, of which 6 were waited for; matrix products, arithmetic and copies ran while one was open for 5% of the time, Pallas kernels for 0%

commit v1 on v0

--- a/solution.py
+++ b/solution.py
@@ -2,6 +2,27 @@
 import jax.numpy as jnp
 from jax import lax
 from jax.sharding import PartitionSpec as P
+
+
+def laid_out(blocks, dim):
+    blocks = jnp.moveaxis(blocks, 0, dim)
+    lengths = blocks.shape
+    return blocks.reshape(*lengths[:dim], lengths[dim] * lengths[dim + 1], *lengths[dim + 2 :])
+
+
+def collected_by_bits(shard, axis):
+    size, index = (lax.axis_size(axis), lax.axis_index(axis))
+    pieces, stride = (shard[None], 1)
+    while stride < size:
+        theirs = lax.ppermute(pieces, axis, [(i, i ^ stride) for i in range(size)])
+        low = index & stride == 0
+        pieces = jnp.concatenate([jnp.where(low, pieces, theirs), jnp.where(low, theirs, pieces)])
+        stride *= 2
+    return pieces
+
+
+def collect(array, axis, dim):
+    return laid_out(collected_by_bits(array, axis), dim)
 
 
 def rms_scale(values_in, gain_vec):
@@ -111,11 +132,7 @@
         state_norm,
         state_max,
     )
-    partial_out = jnp.dot(
-        cell_out,
-        lax.all_gather(w_out, "ep", axis=1, tiled=True),
-        preferred_element_type=jnp.float32,
-    )
+    partial_out = jnp.dot(cell_out, collect(w_out, "ep", 1), preferred_element_type=jnp.float32)
     attended = lax.psum(partial_out.astype(jnp.bfloat16), "tp").astype(jnp.float32)
     resid = (tokens.astype(jnp.float32) + attended).astype(jnp.bfloat16)
     normed_two = rms_scale(resid, ffn_gain).astype(jnp.bfloat16)

time: 343 us -> 312 us (0.910)
  waiting for transfers between devices: 230 us -> 192 us
  other arithmetic: 14.3 us -> 19 us
    all_gather x1 -> x0, waiting for transfers between devices: 39 us -> none  [body(): lax.all_gather(w_out, 'ep', axis=1, tiled=True)]
    ppermute x0 -> x4, waiting for transfers between devices: none -> 38.4 us  [collected_by_bits(): theirs = lax.ppermute(pieces, axis, [(i, i ^ stride) for i in range(size)])]
    reduce_scatter x1, waiting for transfers between devices: 126 us -> 89.6 us  [body(): lax.psum_scatter(jnp.dot(spread, joined, preferred_element_type=jnp.float...]
  transfers between devices with their start and end apart: 6 -> 9, of which waited for: 6 -> 9; matrix products, arithmetic and copies ran while one was open for 5% -> 3% of each run, Pallas kernels for 0% -> 0%
where the time goes in v1:
time: 312 us; the launch traced here: 311 us
  waiting for transfers between devices  192 us (62%)
  blocking collectives  33.1 us (11%)
  matrix products  20.4 us (7%)
  other arithmetic  19 us (6%)
  starting transfers between devices  16.8 us (5%)
  local copies, waits for them, and re-layouts  16.3 us (5%)
  between operations  14 us (4%)
    reduce_scatter x1, waiting for transfers between devices, body(): lax.psum_scatter(jnp.dot(spread, joined, preferred_element_type=jnp.float...  89.6 us
    ppermute x4, waiting for transfers between devices, collected_by_bits(): theirs = lax.ppermute(pieces, axis, [(i, i ^ stride) for i in range(size)])  38.4 us
    all_to_all x1, blocking collectives, body(): lax.all_to_all(outgoing, 'ep', split_axis=0, concat_axis=0, tiled=True)  33.1 us
    all_to_all x1, waiting for transfers between devices, body(): lax.all_to_all(finished, 'ep', split_axis=0, concat_axis=0, tiled=True)  25.1 us
    psum x1, waiting for transfers between devices, body(): expert_sum = lax.psum(partial_down.astype(jnp.bfloat16), 'tp')  17.9 us
    psum x1, waiting for transfers between devices, body(): lax.psum(partial_out.astype(jnp.bfloat16), 'tp').astype(jnp.float32)  17 us
    all_to_all x1, starting transfers between devices, body(): lax.all_to_all(normed, 'ep', split_axis=1, concat_axis=0, tiled=True)  7.22 us
    all_to_all x1, starting transfers between devices, body(): lax.all_to_all(finished, 'ep', split_axis=0, concat_axis=0, tiled=True)  7.11 us
  transfers between devices with their start and end apart: 9, of which 9 were waited for; matrix products, arithmetic and copies ran while one was open for 3% of the time, Pallas kernels for 0%

profile of v1, /device:TPU:8, one launch (start us, length us, event | category | flops | bytes accessed | tf_op | source)
XLA Modules:
  0.0 311.4 jit_solution(2639817749791169274)
XLA Ops:
  7.2 1.2 fusion.36
  8.4 1.7 copy_bitcast_fusion
  10.1 7.2 %all-to-all-start = ((bf16[32,16,128]{2,0,1:T(8,128)(2,1)}), bf16[32,16,128]{2,0,1:T(8,128)(2,1)S(1)}, u32[]{:S(2)}, u32[]{:S(2)}) async-start(bf16[32,16,128]{2,0,1:T(8,128)(2,1)} %copy_bitcast_fusion), calls=%async_computation | async-start | bytes 262144 | tf_op jit(solution)/shard_map/all_to_all | solution.py:103
  17.3 0.8 copy.60
  18.1 0.8 copy.61
  18.9 1.1 concatenate.15
  20.0 3.9 %all-to-all-done = bf16[32,16,128]{2,0,1:T(8,128)(2,1)S(1)} async-done(((bf16[32,16,128]{2,0,1:T(8,128)(2,1)}), bf16[32,16,128]{2,0,1:T(8,128)(2,1)S(1)}, u32[]{:S(2)}, u32[]{:S(2)}) %all-to-all-start) | async-done | bytes 131104 | tf_op jit(solution)/shard_map/all_to_all | solution.py:103
  23.9 1.9 fusion.62
  25.8 0.1 copy.63
  25.9 0.6 collective-permute-start
  26.6 3.7 %collective-permute-done = bf16[1,256,128]{1,2,0:T(8,128)(2,1)S(1)} collective-permute-done((bf16[1,256,128]{1,2,0:T(8,128)(2,1)S(1)}, bf16[1,256,128]{1,2,0:T(8,128)(2,1)S(1)}, u32[]{:S(2)}, u32[]{:S(2)}) %collective-permute-start) | collective-permute-done | bytes 65568 | tf_op jit(solution)/shard_map/ppermute | solution.py:17
  30.3 0.8 collective-permute-start.1
  31.1 5.3 %collective-permute-done.1 = bf16[2,256,128]{1,2,0:T(8,128)(2,1)S(1)} collective-permute-done((bf16[2,256,128]{1,2,0:T(8,128)(2,1)S(1)}, bf16[2,256,128]{1,2,0:T(8,128)(2,1)S(1)}, u32[]{:S(2)}, u32[]{:S(2)}) %collective-permute-start.1) | collective-permute-done | bytes 131104 | tf_op jit(solution)/shard_map/ppermute | solution.py:17
  36.4 0.6 copy-done.4
  37.1 0.9 collective-permute-start.2
  38.0 7.4 %collective-permute-done.2 = bf16[4,256,128]{1,2,0:T(8,128)(2,1)} collective-permute-done((bf16[4,256,128]{1,2,0:T(8,128)(2,1)S(1)}, bf16[4,256,128]{1,2,0:T(8,128)(2,1)}, u32[]{:S(2)}, u32[]{:S(2)}) %collective-permute-start.2) | collective-permute-done | bytes 262176 | tf_op jit(solution)/shard_map/ppermute | solution.py:17
  45.3 1.0 broadcast_select_fusion.3
  46.4 0.8 pad_maximum_fusion.1
  47.2 0.1 copy.62
  47.3 0.1 copy.64
  47.4 0.1 eq.66
  47.6 0.1 reduce_window_sum.11
  47.8 0.7 select_reduce_fusion
  48.5 22.0 %collective-permute-done.3 = bf16[8,256,128]{1,2,0:T(8,128)(2,1)} collective-permute-done((bf16[8,256,128]{1,2,0:T(8,128)(2,1)}, bf16[8,256,128]{1,2,0:T(8,128)(2,1)}, u32[]{:S(2)}, u32[]{:S(2)}) %collective-permute-start.3) | collective-permute-done | bytes 524320 | tf_op jit(solution)/shard_map/ppermute | solution.py:17
  70.5 1.1 broadcast_select_fusion.1
  71.6 1.1 pad_maximum_fusion
  72.6 89.6 %reduce-scatter.2.cloned.1.call-done = f32[32,1032]{1,0:T(8,128)} async-done(((f32[512,1032]{1,0:T(8,128)}), f32[32,1032]{1,0:T(8,128)}) %reduce-scatter.2.cloned.1.call-update) | async-done | bytes 132112 | tf_op jit(solution)/shard_map/reduce_scatter | solution.py:105
  162.3 0.9 convert.9
  163.2 0.1 reshape.153
  163.3 0.1 reshape.175
  163.4 0.1 reshape.167
  163.5 0.1 reshape.165
  163.6 0.9 broadcast_multiply_fusion.3
  164.5 0.8 subtract_exponential_fusion.1
  165.3 0.8 multiply_reduce_fusion.1
  166.1 3.8 %multiply_add_fusion = f32[32,4,64,64]{3,2,1,0:T(8,128)S(1)} fusion(f32[32,4,64,64]{3,2,1,0:T(8,128)} %param.33, f32[32,4,64]{2,1,0:T(4,128)S(1)} %get-tuple-element.38, f32[32,4,64]{2,1,0:T(4,128)S(1)} %get-tuple-element.39, f32[32,4]{1,0:T(8,128)S(1)} %subtract_exponential_fusion.1), kind=kLoop, calls=%fused_computation | loop fusion | flops 1572864 | bytes 4260352 | tf_op jit(solution)/shard_map/add | solution.py:59
  169.9 2.0 copy-done.1
  172.0 3.4 %fusion.63 = f32[32,4,1,64]{3,2,1,0:T(1,128)S(1)} fusion(f32[32,4,64,64]{3,2,1,0:T(8,128)S(1)} %multiply_add_fusion, bf16[32,4,64,1]{2,3,1,0:T(2,128)(2,1)S(1)} %reshape.175), kind=kOutput, calls=%fused_computation.96 | convolution fusion | flops 6291456 | bytes 2146304 | tf_op jit(solution)/shard_map/bhvd,bhd->bhv/dot_general | solution.py:63
  175.3 0.2 fusion.59
  175.5 0.2 multiply_reduce_fusion
  175.7 0.1 subtract_multiply_fusion
  175.9 0.1 reshape.155
  176.0 2.3 convolution_convert_fusion.1
  178.4 0.6 multiply_add_fusion.3
  179.0 17.0 %all-reduce.3.cloned.1.call-done = bf16[32,2048]{1,0:T(8,128)(2,1)} async-done(((bf16[32,2048]{1,0:T(8,128)(2,1)}), bf16[32,2048]{1,0:T(8,128)(2,1)}) %all-reduce.3.cloned.1.call-update) | async-done | bytes 131088 | tf_op jit(solution)/shard_map/psum | solution.py:136
  195.9 1.1 fusion.40
  197.0 1.0 fusion.42
  198.0 0.2 broadcast_in_dim.5
  198.2 1.1 reshape.157
  199.3 2.4 convolution_convert_fusion
  201.7 2.1 reshape.158
  203.9 33.1 %all_to_all.29 = bf16[16,12,2048]{2,1,0:T(8,128)(2,1)S(1)} all-to-all(bf16[16,12,2048]{2,1,0:T(8,128)(2,1)} %reshape.158), channel_id=1, replica_groups=mesh['ep'=16,'tp'=2] {'ep'}, dimensions={0} | all-to-all | bytes 1572864 | tf_op jit(solution)/shard_map/all_to_all | solution.py:159
  237.0 1.0 copy-done.5
  237.9 3.8 %fusion.9 = f32[16,1,12,704]{3,0,2,1:T(8,128)} fusion(bf16[1,2048,704]{1,2,0:T(8,128)(2,1)} %param.37, bf16[16,12,2048]{2,1,0:T(8,128)(2,1)S(1)} %all_to_all.29), kind=kOutput, calls=%fused_computation.11 | convolution fusion | flops 553648128 | bytes 4210688 | tf_op jit(solution)/shard_map/nxcd,xdf->nxcf/dot_general | solution.py:162
  241.7 5.2 %fusion.6 = bf16[16,12,2048]{2,0,1:T(8,128)(2,1)} fusion(bf16[1,704,2048]{2,1,0:T(8,128)(2,1)S(1)} %copy-done, bf16[1,2048,704]{1,2,0:T(8,128)(2,1)} %param.38, f32[16,1,12,704]{3,0,2,1:T(8,128)} %fusion.9, bf16[16,12,2048]{2,1,0:T(8,128)(2,1)} %copy-done.5), kind=kOutput, calls=%fused_computation.7 | convolution fusion | flops 1108500480 | bytes 7880704 | tf_op jit(solution)/shard_map/nxcf,xfd->nxcd/dot_general | solution.py:169
  247.0 17.9 %all-reduce.5.cloned.1.call-done = bf16[16,12,2048]{2,0,1:T(8,128)(2,1)} async-done(((bf16[16,12,2048]{2,0,1:T(8,128)(2,1)}), bf16[16,12,2048]{2,0,1:T(8,128)(2,1)}) %all-reduce.5.cloned.1.call-update) | async-done | bytes 786448 | tf_op jit(solution)/shard_map/psum | solution.py:172
  264.9 2.6 copy.68
  267.5 7.1 %all-to-all-start.2 = ((bf16[16,12,2048]{2,1,0:T(8,128)(2,1)}), bf16[16,12,2048]{2,1,0:T(8,128)(2,1)}, u32[]{:S(2)}, u32[]{:S(2)}) async-start(bf16[16,12,2048]{2,1,0:T(8,128)(2,1)} %copy.68), calls=%async_computation.3 | async-start | bytes 2097152 | tf_op jit(solution)/shard_map/all_to_all | solution.py:174
  274.6 0.1 reduce_sum.70
  274.8 0.7 copy.69
  275.5 25.1 %all-to-all-done.2 = bf16[16,12,2048]{2,1,0:T(8,128)(2,1)} async-done(((bf16[16,12,2048]{2,1,0:T(8,128)(2,1)}), bf16[16,12,2048]{2,1,0:T(8,128)(2,1)}, u32[]{:S(2)}, u32[]{:S(2)}) %all-to-all-start.2) | async-done | bytes 786464 | tf_op jit(solution)/shard_map/all_to_all | solution.py:174
  300.6 2.2 reshape.173
  302.7 1.5 fusion.18
  304.2 0.7 fusion.43
  (53 shorter events, 0.6 us)
Async XLA Ops:
  7.2 234.6 %copy-start = (bf16[1,704,2048]{2,1,0:T(8,128)(2,1)S(1)}, bf16[1,704,2048]{2,1,0:T(8,128)(2,1)}, u32[]{:S(2)}) copy-start(bf16[1,704,2048]{2,1,0:T(8,128)(2,1)} %param.39) | copy-start | bytes 8650756
  10.1 13.8 %all-to-all-start = ((bf16[32,16,128]{2,0,1:T(8,128)(2,1)}), bf16[32,16,128]{2,0,1:T(8,128)(2,1)S(1)}, u32[]{:S(2)}, u32[]{:S(2)}) async-start(bf16[32,16,128]{2,0,1:T(8,128)(2,1)} %copy_bitcast_fusion), calls=%async_computation | async-start | bytes 262144 | tf_op jit(solution)/shard_map/all_to_all | solution.py:103
  17.3 145.0 %reduce-scatter.2.cloned.1.call-start = ((), (), s32[]{:S(2)}) async-start(), calls=%async_computation.4 | async-start | bytes 2506752 | tf_op jit(solution)/shard_map/reduce_scatter | solution.py:105
  18.9 6.9 %copy-start.7 = (bf16[256,128]{1,0:T(8,128)(2,1)S(1)}, bf16[256,128]{1,0:T(8,128)(2,1)}, u32[]{:S(2)}) copy-start(bf16[256,128]{1,0:T(8,128)(2,1)} %param.32) | copy-start | bytes 196612
  25.7 21.5 %copy-start.16 = (f32[32,4]{0,1:T(4,128)S(1)}, f32[32,4]{0,1:T(4,128)}, u32[]{:S(2)}) copy-start(f32[32,4]{0,1:T(4,128)} %param.35) | copy-start | bytes 1540
  25.7 21.6 %copy-start.9 = (s32[32,3]{0,1:T(4,128)S(1)}, s32[32,3]{0,1:T(4,128)}, u32[]{:S(2)}) copy-start(s32[32,3]{0,1:T(4,128)} %param.40) | copy-start | bytes 1156
  25.8 170.1 %all-reduce.3.cloned.1.call-start = ((), (), s32[]{:S(2)}) async-start(), calls=%async_computation.5 | async-start | bytes 262144 | tf_op jit(solution)/shard_map/psum | solution.py:136
  25.9 4.3 %collective-permute-start = (bf16[1,256,128]{1,2,0:T(8,128)(2,1)S(1)}, bf16[1,256,128]{1,2,0:T(8,128)(2,1)S(1)}, u32[]{:S(2)}, u32[]{:S(2)}) collective-permute-start(bf16[1,256,128]{1,2,0:T(8,128)(2,1)S(1)} %bitcast.79), channel_id=1, source_target_pairs={{0,2},{2,0},{4,6},{6,4},{8,10},{10,8},{12,14},{14,12},{16,18},{18,... | collective-permute-start | bytes 196616 | tf_op jit(solution)/shard_map/ppermute | solution.py:17
  30.3 6.1 %collective-permute-start.1 = (bf16[2,256,128]{1,2,0:T(8,128)(2,1)S(1)}, bf16[2,256,128]{1,2,0:T(8,128)(2,1)S(1)}, u32[]{:S(2)}, u32[]{:S(2)}) collective-permute-start(bf16[2,256,128]{1,2,0:T(8,128)(2,1)S(1)} %pad_maximum_fusion.3), channel_id=1, source_target_pairs={{0,4},{2,6},{4,0},{6,2},{8,12},{10,14},{12,8},{14,10},{16,20},{18,... | collective-permute-start | bytes 393224 | tf_op jit(solution)/shard_map/ppermute | solution.py:17
  36.4 0.7 copy-start.4
  37.1 8.2 %collective-permute-start.2 = (bf16[4,256,128]{1,2,0:T(8,128)(2,1)S(1)}, bf16[4,256,128]{1,2,0:T(8,128)(2,1)}, u32[]{:S(2)}, u32[]{:S(2)}) collective-permute-start(bf16[4,256,128]{1,2,0:T(8,128)(2,1)S(1)} %pad_maximum_fusion.2), channel_id=1, source_target_pairs={{0,8},{2,10},{4,12},{6,14},{8,0},{10,2},{12,4},{14,6},{16,24},{18,... | collective-permute-start | bytes 786440 | tf_op jit(solution)/shard_map/ppermute | solution.py:17
  47.2 23.2 %collective-permute-start.3 = (bf16[8,256,128]{1,2,0:T(8,128)(2,1)}, bf16[8,256,128]{1,2,0:T(8,128)(2,1)}, u32[]{:S(2)}, u32[]{:S(2)}) collective-permute-start(bf16[8,256,128]{1,2,0:T(8,128)(2,1)} %pad_maximum_fusion.1), channel_id=1, source_target_pairs={{0,16},{2,18},{4,20},{6,22},{8,24},{10,26},{12,28},{14,30},{16,0},... | collective-permute-start | bytes 1572872 | tf_op jit(solution)/shard_map/ppermute | solution.py:17
  47.5 116.0 %copy-start.11 = (s32[96]{0:T(128)}, s32[96]{0:T(128)S(1)}, u32[]{:S(2)}) copy-start(s32[96]{0:T(128)S(1)} %eq.66) | copy-start | bytes 1156
  48.5 116.9 %copy-start.6 = (f32[32,4,64]{2,1,0:T(4,128)S(1)}, f32[32,4,64]{2,1,0:T(4,128)}, u32[]{:S(2)}) copy-start(f32[32,4,64]{2,1,0:T(4,128)} %param.34) | copy-start | bytes 98308
  169.9 2.0 copy-start.1
  171.9 4.0 %copy-start.17 = (f32[256]{0:T(256)S(1)}, f32[256]{0:T(256)}, u32[]{:S(2)}) copy-start(f32[256]{0:T(256)} %param.31) | copy-start | bytes 3076
  171.9 6.4 %copy-start.12 = (s32[96]{0:T(128)S(1)}, s32[96]{0:T(128)}, u32[]{:S(2)}) copy-start(s32[96]{0:T(128)} %copy-done.11) | copy-start | bytes 1156
  171.9 6.4 %copy-start.14 = (s32[96]{0:T(128)S(1)}, s32[96]{0:T(128)}, u32[]{:S(2)}) copy-start(s32[96]{0:T(128)} %select_reduce_fusion) | copy-start | bytes 1156
  171.9 24.0 %copy-start.2 = (bf16[32,2048]{1,0:T(8,128)(2,1)S(1)}, bf16[32,2048]{1,0:T(8,128)(2,1)}, u32[]{:S(2)}) copy-start(bf16[32,2048]{1,0:T(8,128)(2,1)} %param.21) | copy-start | bytes 393220
  171.9 25.0 %copy-start.8 = (f32[2048]{0:T(1024)S(1)}, f32[2048]{0:T(1024)}, u32[]{:S(2)}) copy-start(f32[2048]{0:T(1024)} %param.36) | copy-start | bytes 24580
  178.3 86.6 %all-reduce.5.cloned.1.call-start = ((), (), s32[]{:S(2)}) async-start(), calls=%async_computation.6 | async-start | bytes 1572864 | tf_op jit(solution)/shard_map/psum | solution.py:172
  237.0 1.0 copy-start.5
  247.0 27.7 %copy-start.15 = (s32[96]{0:T(128)S(1)}, s32[96]{0:T(128)}, u32[]{:S(2)}) copy-start(s32[96]{0:T(128)} %select_reduce_fusion) | copy-start | bytes 1156
  247.0 27.8 %copy-start.10 = (s32[32,3]{0,1:T(4,128)S(1)}, s32[32,3]{0,1:T(4,128)}, u32[]{:S(2)}) copy-start(s32[32,3]{0,1:T(4,128)} %param.40) | copy-start | bytes 1156
  247.0 55.7 %copy-start.13 = (f32[32,3]{0,1:T(4,128)S(1)}, f32[32,3]{0,1:T(4,128)}, u32[]{:S(2)}) copy-start(f32[32,3]{0,1:T(4,128)} %param.41) | copy-start | bytes 1156
  267.5 36.7 %copy-start.3 = (bf16[32,2048]{1,0:T(8,128)(2,1)S(1)}, bf16[32,2048]{1,0:T(8,128)(2,1)}, u32[]{:S(2)}) copy-start(bf16[32,2048]{1,0:T(8,128)(2,1)} %all-reduce.3.cloned.1.call-done) | copy-start | bytes 393220
  267.5 33.0 %all-to-all-start.2 = ((bf16[16,12,2048]{2,1,0:T(8,128)(2,1)}), bf16[16,12,2048]{2,1,0:T(8,128)(2,1)}, u32[]{:S(2)}, u32[]{:S(2)}) async-start(bf16[16,12,2048]{2,1,0:T(8,128)(2,1)} %copy.68), calls=%async_computation.3 | async-start | bytes 2097152 | tf_op jit(solution)/shard_map/all_to_all | solution.py:174
Sparse Core Ops, SparseCore 0:
  25.9 136.3 reduce-scatter.1
  178.4 17.4 all-reduce.2
  247.1 17.7 all-reduce.4
